TPU v7x, 32 devices: a whole 2x2x4 slice. The times are simulated.
32 devices in a mesh: ep: 16 (over z, y, x), tp: 2 (over core).
Axes of the slice: x: 2, y: 2, z: 4, core: 2. Of those that a mesh axis runs over, the one named last changes fastest.
Arguments:
- tokens: bfloat16 [1024, 2048], P('ep', 'tp'), may hold values from -6 to 6
- sequence_state_real: float32 [1024, 128, 64], P('ep', 'tp'), may hold values from -4 to 4
- sequence_state_imaginary: float32 [1024, 128, 64], P('ep', 'tp'), may hold values from -4 to 4
- mixer_norm_gain: float32 [2048], replicated, may hold values from 0.1 to 1.9
- expert_norm_gain: float32 [2048], replicated, may hold values from 0.1 to 1.9
- rate: float32 [128, 64], P('tp'), may hold values from 0.1 to 4
- freq: float32 [128, 64], P('tp'), may hold values from -3 to 3
- log_group_step: float32 [128], P('tp'), may hold values from -3 to 0
- input_map_real: float32 [128, 64, 16], P('tp'), may hold values from -1 to 1
- input_map_imaginary: float32 [128, 64, 16], P('tp'), may hold values from -1 to 1
- output_map_real: float32 [128, 16, 64], P('tp'), may hold values from -0.75 to 0.75
- output_map_imaginary: float32 [128, 16, 64], P('tp'), may hold values from -0.75 to 0.75
- skip: float32 [2048], P('tp'), may hold values from -4 to 4
- mixer_value_weight: bfloat16 [2048, 2048], P('tp'), may hold values from -0.125 to 0.125
- mixer_gate_weight: bfloat16 [2048, 2048], P('tp'), may hold values from -0.125 to 0.125
- group_router_weight: bfloat16 [2048, 4], replicated, may hold values from -0.125 to 0.125
- expert_router_weight: bfloat16 [2048, 16], replicated, may hold values from -0.125 to 0.125
- dense_blend_weight: float32 [2048], replicated, may hold values from -0.125 to 0.125
- routes: int32 [1024, 2], P('ep'), may hold values from 0 to 15, all different within a row; in each aligned block of 64 rows (0 to 63, 64 to 127, ...) at most 16 rows name the same one
- expert_gate_weight: bfloat16 [16, 2048, 1024], P('ep', None, 'tp'), may hold values from -0.125 to 0.125
- expert_up_weight: bfloat16 [16, 2048, 1024], P('ep', None, 'tp'), may hold values from -0.125 to 0.125
- expert_down_weight: bfloat16 [16, 1024, 2048], P('ep', 'tp'), may hold values from -0.1875 to 0.1875
- shared_gate_weight: bfloat16 [2048, 2048], P('tp', 'ep'), may hold values from -0.125 to 0.125
- shared_up_weight: bfloat16 [2048, 2048], P('tp', 'ep'), may hold values from -0.125 to 0.125
- shared_down_weight: bfloat16 [2048, 2048], P(None, 'tp'), may hold values from -0.125 to 0.125
Outputs:
- result: bfloat16 [1024, 2048], P('ep', 'tp')
- next_re: float32 [1024, 128, 64], P('ep', 'tp')
- next_im: float32 [1024, 128, 64], P('ep', 'tp')
Inputs may be any that keep to these rules, and one draw needn't show every extreme that they name: `routes`: each row names 2 different experts. Among the rows of one device no expert is named more than 16 times, and in every draw some expert is named exactly 16 times by some device's rows.
All inputs are finite; a program needn't handle non-finite values.
Results may differ from a plain program's by a relative error of at most 0.017.
Values may be sent and summed in bfloat16 or wider, within the bound.
A program may use at most 128 MiB of HBM per device.

v0:
```python
import jax
import jax.numpy as jnp
from jax import lax
from jax.sharding import PartitionSpec as P

NG = 4
EPS = 1e-06
PRECISION_MAX = lax.Precision.HIGHEST


def state_factors(rate, freq, log_group_step, input_map_real, input_map_imaginary):
    step_size = jnp.exp(log_group_step)[:, None]
    magnitude = jnp.exp(-rate * step_size)
    abar_re = magnitude * jnp.cos(freq * step_size)
    abar_im = magnitude * jnp.sin(freq * step_size)
    denom = rate * rate + freq * freq
    shift_re = abar_re - 1.0
    fac_re = (abar_im * freq - shift_re * rate) / denom
    fac_im = -(abar_im * rate + shift_re * freq) / denom
    bbar_re = fac_re[:, :, None] * input_map_real - fac_im[:, :, None] * input_map_imaginary
    bbar_im = fac_re[:, :, None] * input_map_imaginary + fac_im[:, :, None] * input_map_real
    return (abar_re, abar_im, bbar_re, bbar_im)


def state_step(
    normed,
    sequence_state_real,
    sequence_state_imaginary,
    factors,
    output_map_real,
    output_map_imaginary,
    skip,
):
    abar_re, abar_im, bbar_re, bbar_im = factors
    groups = abar_re.shape[0]
    inputs = normed.astype(jnp.float32)
    grouped = inputs.reshape(inputs.shape[0], groups, -1)
    drive_re = jnp.einsum("tgc,gpc->tgp", grouped, bbar_re, precision=PRECISION_MAX)
    drive_im = jnp.einsum("tgc,gpc->tgp", grouped, bbar_im, precision=PRECISION_MAX)
    fresh_real = abar_re * sequence_state_real - abar_im * sequence_state_imaginary + drive_re
    fresh_imaginary = abar_re * sequence_state_imaginary + abar_im * sequence_state_real + drive_im
    state_readout = jnp.einsum("dor,zdr->zdo", output_map_real, fresh_real, precision=PRECISION_MAX)
    state_readout = state_readout - jnp.einsum(
        "dor,zdr->zdo", output_map_imaginary, fresh_imaginary, precision=PRECISION_MAX
    )
    mixed = state_readout.reshape(inputs.shape) + skip * inputs
    return (mixed, fresh_real, fresh_imaginary)


def pair_product(left, first_map, second_map):
    first = jnp.dot(left, first_map, preferred_element_type=jnp.float32)
    second = jnp.dot(left, second_map, preferred_element_type=jnp.float32)
    return jnp.concatenate([first, second], axis=1)


def shards(
    tokens,
    sequence_state_real,
    sequence_state_imaginary,
    mixer_norm_gain,
    expert_norm_gain,
    rate,
    freq,
    log_group_step,
    input_map_real,
    input_map_imaginary,
    output_map_real,
    output_map_imaginary,
    skip,
    mixer_value_weight,
    mixer_gate_weight,
    group_router_weight,
    expert_router_weight,
    dense_blend_weight,
    routes,
    expert_gate_weight,
    expert_up_weight,
    expert_down_weight,
    shared_gate_weight,
    shared_up_weight,
    shared_down_weight,
):
    seq_rows, half_width = tokens.shape
    width = 2 * half_width
    column_start = lax.axis_index("tp") * half_width

    def own_rows(values):
        return lax.dynamic_slice_in_dim(values, column_start, half_width, 0)

    float_tokens = tokens.astype(jnp.float32)
    square_sum = lax.psum(jnp.sum(float_tokens * float_tokens, axis=1), "tp")
    first_scale = lax.rsqrt(square_sum / width + EPS)[:, None]
    normed = (float_tokens * first_scale * own_rows(mixer_norm_gain)).astype(jnp.bfloat16)
    factors = state_factors(rate, freq, log_group_step, input_map_real, input_map_imaginary)
    mixed, next_re, next_im = state_step(
        normed,
        sequence_state_real,
        sequence_state_imaginary,
        factors,
        output_map_real,
        output_map_imaginary,
        skip,
    )
    activated = jax.nn.gelu(mixed).astype(jnp.bfloat16)
    value_part = jnp.dot(activated, mixer_value_weight, preferred_element_type=jnp.float32)
    gate_part = jnp.dot(activated, mixer_gate_weight, preferred_element_type=jnp.float32)
    stacked = jnp.stack([value_part, gate_part], axis=1)
    mix_sum = lax.psum_scatter(
        stacked.astype(jnp.bfloat16), "tp", scatter_dimension=2, tiled=True
    ).astype(jnp.float32)
    mix_half = (mix_sum[:, 0] * jax.nn.sigmoid(mix_sum[:, 1])).astype(jnp.bfloat16)
    hidden = (float_tokens + mix_half.astype(jnp.float32)).astype(jnp.bfloat16)
    hidden_f32 = hidden.astype(jnp.float32)
    scaled = hidden_f32 * own_rows(expert_norm_gain)
    router_map = jnp.concatenate(
        [own_rows(group_router_weight), own_rows(expert_router_weight)], axis=1
    ).astype(jnp.float32)
    blend_map = own_rows(dense_blend_weight)
    hidden_squares = jnp.sum(hidden_f32 * hidden_f32, axis=1)
    total_squares = lax.psum(hidden_squares, "tp")
    inverse = lax.rsqrt(total_squares / width + EPS)[:, None]
    normal_rows = scaled * inverse
    raw_part = jnp.dot(normal_rows, router_map, precision=PRECISION_MAX)
    blend_part = jnp.dot(normal_rows, blend_map, precision=PRECISION_MAX)
    logits, blend_logit = lax.psum((raw_part, blend_part), "tp")
    hnorm = (scaled * inverse).astype(jnp.bfloat16)
    experts = expert_router_weight.shape[1]
    top_count = routes.shape[1]
    per_group = experts // NG
    group_prob = jax.nn.softmax(logits[:, :NG], axis=-1)
    expert_logits = logits[:, NG:]
    expert_hits = routes[:, :, None] == jnp.arange(experts, dtype=jnp.int32)[None, None, :]
    chosen = jnp.sum(jnp.where(expert_hits, expert_logits[:, None, :], 0.0), axis=2)
    group_hits = (routes // per_group)[:, :, None] == jnp.arange(NG, dtype=jnp.int32)[None, None, :]
    group_sel = jnp.sum(jnp.where(group_hits, group_prob[:, None, :], 0.0), axis=2)
    weights = jax.nn.softmax(chosen, axis=1) * group_sel
    full_rows = lax.all_gather(hnorm, "tp", axis=1, tiled=True)
    capacity = max(2, 2 * seq_rows * top_count // experts)
    flat_routes = routes.reshape(-1)
    matches = (flat_routes[:, None] == jnp.arange(experts, dtype=jnp.int32)[None, :]).astype(
        jnp.int32
    )
    slot_rank = jnp.sum(jnp.cumsum(matches, axis=0) * matches, axis=1) - 1
    slot_target = flat_routes * capacity + slot_rank
    dispatch = slot_target[None, :] == jnp.arange(experts * capacity, dtype=jnp.int32)[:, None]
    dispatch_rows = jnp.sum(
        dispatch.reshape(experts * capacity, seq_rows, top_count).astype(jnp.float32), axis=2
    )
    outgoing = jnp.dot(
        dispatch_rows.astype(jnp.bfloat16), full_rows, preferred_element_type=jnp.float32
    )
    outgoing = outgoing.astype(jnp.bfloat16).reshape(experts, capacity, width)
    received = lax.all_to_all(outgoing, "ep", split_axis=0, concat_axis=0, tiled=True)
    sources = received.shape[0]
    items = received.shape[1]
    token_rows = received.reshape(sources * items, width)
    gate_e = jnp.dot(token_rows, expert_gate_weight[0], preferred_element_type=jnp.float32)
    expert_up_rows = jnp.dot(token_rows, expert_up_weight[0], preferred_element_type=jnp.float32)
    inner = (jax.nn.silu(gate_e) * expert_up_rows).astype(jnp.bfloat16)
    part_out = jnp.dot(inner, expert_down_weight[0], preferred_element_type=jnp.float32)
    total = lax.psum_scatter(part_out.astype(jnp.bfloat16), "tp", scatter_dimension=1, tiled=True)
    finished = total.reshape(sources, items, half_width)
    returned = lax.all_to_all(finished, "ep", split_axis=0, concat_axis=0, tiled=True)
    returned_flat = returned.reshape(experts * capacity, half_width)
    picked = returned_flat[slot_target].reshape(seq_rows, top_count, half_width).astype(jnp.float32)
    routed = jnp.sum(weights[:, :, None] * picked, axis=1)
    partial_dense = pair_product(
        lax.all_gather(hnorm, "ep", axis=0, tiled=True), shared_gate_weight, shared_up_weight
    )
    dense_sum = lax.psum(partial_dense.astype(jnp.bfloat16), "tp").astype(jnp.float32)
    dense_cols = shared_gate_weight.shape[1]
    inner_cols = (jax.nn.silu(dense_sum[:, :dense_cols]) * dense_sum[:, dense_cols:]).astype(
        jnp.bfloat16
    )
    dense_inner = lax.all_to_all(inner_cols, "ep", split_axis=0, concat_axis=1, tiled=True)
    dense_out = jnp.dot(dense_inner, shared_down_weight, preferred_element_type=jnp.float32)
    result = hidden_f32 + routed + jax.nn.sigmoid(blend_logit)[:, None] * dense_out
    return (result.astype(jnp.bfloat16), next_re, next_im)


def solution(mesh):
    placed = (
        P("ep", "tp"),
        P("ep", "tp", None),
        P("ep", "tp", None),
        P(),
        P(),
        P("tp", None),
        P("tp", None),
        P("tp"),
        P("tp", None, None),
        P("tp", None, None),
        P("tp", None, None),
        P("tp", None, None),
        P("tp"),
        P("tp", None),
        P("tp", None),
        P(),
        P(),
        P(),
        P("ep", None),
        P("ep", None, "tp"),
        P("ep", None, "tp"),
        P("ep", "tp", None),
        P("tp", "ep"),
        P("tp", "ep"),
        P(None, "tp"),
    )
    return jax.shard_map(
        shards,
        mesh=mesh,
        in_specs=placed,
        out_specs=(P("ep", "tp"), P("ep", "tp", None), P("ep", "tp", None)),
        check_vma=False,
    )
```

profile of v0, /device:TPU:0, one launch (start us, length us, event | category | flops | bytes accessed | tf_op | source)
XLA Modules:
  0.0 187.7 jit_solution(3510667995029894204)
XLA Ops:
  7.2 3.5 %copy.64 = f32[64,64,64]{0,2,1:T(8,128)} copy(f32[64,64,64]{2,1,0:T(8,128)} %param.27) | data formatting | bytes 2097152 | tf_op args[2]
  10.7 3.4 %copy.63 = f32[64,64,64]{0,2,1:T(8,128)} copy(f32[64,64,64]{2,1,0:T(8,128)} %param.26) | data formatting | bytes 2097152 | tf_op args[1]
  14.3 2.6 %psum.35 = f32[64]{0:T(128)S(1)} all-reduce(f32[64]{0:T(128)S(1)} %fusion.29), channel_id=1, replica_groups=mesh['ep'=16,'tp'=2] {'tp'}, use_global_device_ids=true, to_apply=%region_1.0 | all-reduce | flops 64 | bytes 512 | tf_op jit(solution)/shard_map/psum | solution.py:91
  17.7 1.1 copy.65
  18.8 1.0 fusion.68
  19.8 4.9 %bitcast_add_fusion.1 = f32[64,64,64]{0,2,1:T(8,128)S(1)} fusion(f32[64,64,64]{0,2,1:T(8,128)} %copy.64, f32[64,64,64]{0,2,1:T(8,128)} %copy.63, bf16[64,64,16]{0,2,1:T(8,128)(2,1)S(1)} %bitcast.75, f32[64,64]{1,0:T(8,128)S(1)} %get-tuple-element.17, f32[64,64]{1,0:T(8,128)S(1)} %get-tuple-element.18, f32[64,64,16]{1,2,0:T(8,128)S(1)} %copy-done.7, ...), kind=kOutput, calls=%fused_computation.13 | convolution fusion | flops 51576832 | bytes 3866624 | tf_op jit(solution)/shard_map/tgc,gpc->tgp/dot_general | solution.py:38
  24.8 3.2 %bitcast_add_fusion = f32[64,64,64]{0,2,1:T(8,128)S(1)} fusion(f32[64,64,64]{0,2,1:T(8,128)S(1)} %copy-done.4, f32[64,64,64]{0,2,1:T(8,128)S(1)} %copy-done.3, bf16[64,64,16]{0,2,1:T(8,128)(2,1)S(1)} %bitcast.76, f32[64,64]{1,0:T(8,128)S(1)} %get-tuple-element.17, f32[64,64]{1,0:T(8,128)S(1)} %get-tuple-element.18, f32[64,64,16]{1,2,0:T(8,128)S(1)} %copy-done.8, ...), kind=kOutput, calls=%fused_computation.12 | convolution fusion | flops 51576832 | bytes 3866624 | tf_op jit(solution)/shard_map/tgc,gpc->tgp/dot_general | solution.py:39
  28.1 1.9 %fusion.77 = f32[64,64,16]{1,2,0:T(8,128)S(1)} fusion(f32[64,64,64]{0,2,1:T(8,128)S(1)} %bitcast_add_fusion.1, f32[64,16,64]{2,1,0:T(8,128)S(1)} %copy-done.11), kind=kOutput, calls=%fused_computation.123 | convolution fusion | flops 50331648 | bytes 1572864 | tf_op jit(solution)/shard_map/dor,zdr->zdo/dot_general | solution.py:42
  30.0 1.9 %convolution_subtract_fusion = f32[64,64,16]{1,2,0:T(8,128)S(1)} fusion(f32[64,64,16]{1,2,0:T(8,128)S(1)} %fusion.77, f32[64,64,64]{0,2,1:T(8,128)S(1)} %bitcast_add_fusion, f32[64,16,64]{2,1,0:T(8,128)S(1)} %copy-done.10), kind=kOutput, calls=%fused_computation.15 | convolution fusion | flops 50397184 | bytes 1835008 | tf_op jit(solution)/shard_map/dor,zdr->zdo/dot_general | solution.py:43
  32.1 3.3 %fusion.1 = bf16[64,1,2048]{2,0,1:T(8,128)(2,1)S(1)} fusion(bf16[1024,2048]{1,0:T(8,128)(2,1)} %param.39, f32[64,1024]{1,0:T(8,128)S(1)} %copy.70, f32[1024]{0:T(1024)S(1)} %copy-done.14, f32[1024]{0:T(1024)S(1)} %dynamic_slice.15, f32[64]{0:T(128)S(1)} %add_rsqrt_fusion.1, bf16[64,1024]{1,0:T(8,128)(2,1)S(1)} %copy-done.6), kind=kOutput, calls=%fused_computation.6 | convolution fusion | flops 269615104 | bytes 4858112 | tf_op jit(solution)/shard_map/dot_general | solution.py:106
  35.6 1.0 fusion
  37.8 10.3 %reduce-scatter.3.cloned.1.call-done = bf16[64,2,1024]{2,0,1:T(8,128)(2,1)} async-done(((bf16[64,2,2048]{2,0,1:T(8,128)(2,1)}), bf16[64,2,1024]{2,0,1:T(8,128)(2,1)}) %reduce-scatter.3.cloned.1.call-update) | async-done | bytes 262160 | tf_op jit(solution)/shard_map/reduce_scatter | solution.py:108
  48.1 1.0 convert_element_type.70
  49.3 2.5 %psum.36 = f32[64]{0:T(128)S(1)} all-reduce(f32[64]{0:T(128)S(1)} %get-tuple-element.14), channel_id=1, replica_groups=mesh['ep'=16,'tp'=2] {'tp'}, use_global_device_ids=true, to_apply=%region_4.0 | all-reduce | flops 64 | bytes 512 | tf_op jit(solution)/shard_map/psum | solution.py:120
  53.4 2.3 %all_gather.6 = bf16[64,2048]{1,0:T(8,128)(2,1)S(1)} all-gather(bf16[64,1024]{1,0:T(8,128)(2,1)} %fusion.43), channel_id=1, replica_groups=mesh['ep'=16,'tp'=2] {'tp'}, dimensions={1}, use_global_device_ids=true | all-gather | bytes 393216 | tf_op jit(solution)/shard_map/all_gather | solution.py:137
  56.2 41.0 %all_to_all.29 = bf16[16,16,2048]{2,1,0:T(8,128)(2,1)S(1)} all-to-all(bf16[16,16,2048]{2,1,0:T(8,128)(2,1)S(1)} %bitcast.74), channel_id=1, replica_groups=mesh['ep'=16,'tp'=2] {'ep'}, dimensions={0} | all-to-all | bytes 2097152 | tf_op jit(solution)/shard_map/all_to_all | solution.py:153
  97.2 1.0 copy-done.9
  98.9 4.2 %convolution_convert_fusion = bf16[256,2048]{1,0:T(8,128)(2,1)} fusion(bf16[1,512,2048]{2,1,0:T(8,128)(2,1)S(1)} %copy-done, bf16[256,2048]{1,0:T(8,128)(2,1)} %bitcast.79, bf16[1,2048,512]{2,1,0:T(8,128)(2,1)} %param.45, f32[256,512]{1,0:T(8,128)S(1)} %fusion.5), kind=kOutput, calls=%fused_computation.1 | convolution fusion | flops 1075052544 | bytes 6815744 | tf_op jit(solution)/shard_map/dot_general | solution.py:160
  103.1 3.8 %copy.77 = f32[64,64,64]{2,1,0:T(8,128)} copy(f32[64,64,64]{0,2,1:T(8,128)} %copy-done.2) | data formatting | bytes 2097152
  106.9 3.8 %copy.78 = f32[64,64,64]{2,1,0:T(8,128)} copy(f32[64,64,64]{0,2,1:T(8,128)} %copy-done.1) | data formatting | bytes 2097152
  111.7 3.3 %all-reduce = (f32[64,20]{0,1:T(8,128)S(1)}, f32[64]{0:T(128)S(1)}) all-reduce(f32[64,20]{0,1:T(8,128)S(1)} %fusion.44, f32[64]{0:T(128)S(1)} %convolution_bitcast_fusion), channel_id=1, replica_groups=mesh['ep'=16,'tp'=2] {'tp'}, use_global_device_ids=true, to_apply=%region_5.0 | all-reduce | flops 1344 | bytes 10752 | tf_op jit(solution)/shard_map/psum | solution.py:125
  115.1 3.4 %all-gather.2.cloned.1.call-done = bf16[1024,1024]{1,0:T(8,128)(2,1)} async-done(((bf16[64,1024]{1,0:T(8,128)(2,1)}), bf16[1024,1024]{1,0:T(8,128)(2,1)}) %all-gather.2.cloned.1.call-update) | async-done | bytes 2097168 | tf_op jit(solution)/shard_map/all_gather | solution.py:168
  118.5 2.4 %convolution_convert_fusion.4 = bf16[1024,128]{0,1:T(8,128)(2,1)S(1)} fusion(bf16[1024,1024]{1,0:T(8,128)(2,1)} %all-gather.2.cloned.1.call-done, bf16[1024,128]{1,0:T(8,128)(2,1)S(1)} %copy-done.12), kind=kOutput, calls=%fused_computation.17 | convolution fusion | flops 268566528 | bytes 2621440 | tf_op jit(solution)/shard_map/dot_general | solution.py:52
  120.9 7.1 %reduce-scatter.5.cloned.1.call-done = bf16[256,1024]{1,0:T(8,128)(2,1)} async-done(((bf16[256,2048]{1,0:T(8,128)(2,1)}), bf16[256,1024]{1,0:T(8,128)(2,1)}) %reduce-scatter.5.cloned.1.call-update) | async-done | bytes 524304 | tf_op jit(solution)/shard_map/reduce_scatter | solution.py:161
  128.0 6.8 %all-to-all-start.1 = ((bf16[16,16,1024]{2,1,0:T(8,128)(2,1)}), bf16[16,16,1024]{2,1,0:T(8,128)(2,1)S(1)}, u32[]{:S(2)}, u32[]{:S(2)}) async-start(bf16[16,16,1024]{2,1,0:T(8,128)(2,1)} %bitcast.80), calls=%async_computation.3 | async-start | bytes 1048576 | tf_op jit(solution)/shard_map/all_to_all | solution.py:163
  134.9 2.4 %convolution_convert_fusion.5 = bf16[1024,128]{0,1:T(8,128)(2,1)S(1)} fusion(bf16[1024,1024]{1,0:T(8,128)(2,1)} %all-gather.2.cloned.1.call-done, bf16[1024,128]{1,0:T(8,128)(2,1)S(1)} %copy-done.13), kind=kOutput, calls=%fused_computation.18 | convolution fusion | flops 268566528 | bytes 2621440 | tf_op jit(solution)/shard_map/dot_general | solution.py:51
  138.2 20.0 %all-reduce.3.cloned.1.call-done = bf16[1024,256]{0,1:T(8,128)(2,1)} async-done(((bf16[1024,256]{0,1:T(8,128)(2,1)}), bf16[1024,256]{0,1:T(8,128)(2,1)}) %all-reduce.3.cloned.1.call-update) | async-done | bytes 524304 | tf_op jit(solution)/shard_map/psum | solution.py:170
  158.2 1.1 convert_element_type.84
  160.3 6.8 %all-to-all-start.2 = ((bf16[16,64,128]{2,1,0:T(8,128)(2,1)}), bf16[16,64,128]{2,1,0:T(8,128)(2,1)S(1)}, u32[]{:S(2)}, u32[]{:S(2)}) async-start(bf16[16,64,128]{2,1,0:T(8,128)(2,1)} %bitcast.19), calls=%async_computation.4 | async-start | bytes 524288 | tf_op jit(solution)/shard_map/all_to_all | solution.py:175
  167.3 0.9 gather_fusion
  169.2 8.2 %all-to-all-done.2 = bf16[16,64,128]{2,1,0:T(8,128)(2,1)S(1)} async-done(((bf16[16,64,128]{2,1,0:T(8,128)(2,1)}), bf16[16,64,128]{2,1,0:T(8,128)(2,1)S(1)}, u32[]{:S(2)}, u32[]{:S(2)}) %all-to-all-start.2) | async-done | bytes 262176 | tf_op jit(solution)/shard_map/all_to_all | solution.py:175
  177.5 3.7 %fusion.14 = bf16[64,1024]{1,0:T(8,128)(2,1)} fusion(bf16[2048,1024]{1,0:T(8,128)(2,1)} %param.49, f32[64,1024]{1,0:T(8,128)S(1)} %multiply_reduce_fusion, bf16[64,1024]{1,0:T(8,128)(2,1)S(1)} %get-tuple-element.15, f32[64]{0:T(128)S(1)} %add_divide_fusion, bf16[16,64,128]{2,1,0:T(8,128)(2,1)S(1)} %all-to-all-done.2), kind=kOutput, calls=%fused_computation.21 | convolution fusion | flops 268763136 | bytes 4980992 | tf_op jit(solution)/shard_map/dot_general | solution.py:176
  (101 shorter events, 9.5 us)
Async XLA Ops:
  7.2 91.7 %copy-start = (bf16[1,512,2048]{2,1,0:T(8,128)(2,1)S(1)}, bf16[1,512,2048]{2,1,0:T(8,128)(2,1)}, u32[]{:S(2)}) copy-start(bf16[1,512,2048]{2,1,0:T(8,128)(2,1)} %param.46) | copy-start | bytes 6291460
  7.2 40.9 %reduce-scatter.3.cloned.1.call-start = ((), (), s32[]{:S(2)}) async-start(), calls=%async_computation.5 | async-start | bytes 786432 | tf_op jit(solution)/shard_map/reduce_scatter | solution.py:108
  10.7 3.4 %copy-start.6 = (bf16[64,1024]{1,0:T(8,128)(2,1)S(1)}, bf16[64,1024]{1,0:T(8,128)(2,1)}, u32[]{:S(2)}) copy-start(bf16[64,1024]{1,0:T(8,128)(2,1)} %param.25) | copy-start | bytes 393220
  10.7 6.2 %copy-start.18 = (f32[2048]{0:T(1024)S(1)}, f32[2048]{0:T(1024)}, u32[]{:S(2)}) copy-start(f32[2048]{0:T(1024)} %param.28) | copy-start | bytes 24580
  10.7 8.0 %copy-start.21 = (f32[64]{0:T(128)S(1)}, f32[64]{0:T(128)}, u32[]{:S(2)}) copy-start(f32[64]{0:T(128)} %param.32) | copy-start | bytes 772
  10.7 9.1 %copy-start.7 = (f32[64,64,16]{1,2,0:T(8,128)S(1)}, f32[64,64,16]{1,2,0:T(8,128)}, u32[]{:S(2)}) copy-start(f32[64,64,16]{1,2,0:T(8,128)} %param.34) | copy-start | bytes 786436
  10.7 9.1 %copy-start.8 = (f32[64,64,16]{1,2,0:T(8,128)S(1)}, f32[64,64,16]{1,2,0:T(8,128)}, u32[]{:S(2)}) copy-start(f32[64,64,16]{1,2,0:T(8,128)} %param.33) | copy-start | bytes 786436
  19.8 5.0 %copy-start.3 = (f32[64,64,64]{0,2,1:T(8,128)S(1)}, f32[64,64,64]{0,2,1:T(8,128)}, u32[]{:S(2)}) copy-start(f32[64,64,64]{0,2,1:T(8,128)} %copy.64) | copy-start | bytes 3145732
  19.8 5.0 %copy-start.4 = (f32[64,64,64]{0,2,1:T(8,128)S(1)}, f32[64,64,64]{0,2,1:T(8,128)}, u32[]{:S(2)}) copy-start(f32[64,64,64]{0,2,1:T(8,128)} %copy.63) | copy-start | bytes 3145732
  24.8 3.3 %copy-start.2 = (f32[64,64,64]{0,2,1:T(8,128)}, f32[64,64,64]{0,2,1:T(8,128)S(1)}, u32[]{:S(2)}) copy-start(f32[64,64,64]{0,2,1:T(8,128)S(1)} %bitcast_add_fusion.1) | copy-start | bytes 3145732
  24.8 3.3 %copy-start.11 = (f32[64,16,64]{2,1,0:T(8,128)S(1)}, f32[64,16,64]{2,1,0:T(8,128)}, u32[]{:S(2)}) copy-start(f32[64,16,64]{2,1,0:T(8,128)} %param.35) | copy-start | bytes 786436
  28.0 3.9 %copy-start.1 = (f32[64,64,64]{0,2,1:T(8,128)}, f32[64,64,64]{0,2,1:T(8,128)S(1)}, u32[]{:S(2)}) copy-start(f32[64,64,64]{0,2,1:T(8,128)S(1)} %bitcast_add_fusion) | copy-start | bytes 3145732
  28.0 1.9 %copy-start.10 = (f32[64,16,64]{2,1,0:T(8,128)S(1)}, f32[64,16,64]{2,1,0:T(8,128)}, u32[]{:S(2)}) copy-start(f32[64,16,64]{2,1,0:T(8,128)} %param.36) | copy-start | bytes 786436
  30.0 2.1 %copy-start.14 = (f32[1024]{0:T(1024)S(1)}, f32[1024]{0:T(1024)}, u32[]{:S(2)}) copy-start(f32[1024]{0:T(1024)} %param.37) | copy-start | bytes 12292
  32.1 3.5 %copy-start.5 = (bf16[1024,2048]{1,0:T(8,128)(2,1)S(1)}, bf16[1024,2048]{1,0:T(8,128)(2,1)}, u32[]{:S(2)}) copy-start(bf16[1024,2048]{1,0:T(8,128)(2,1)} %param.38) | copy-start | bytes 12582916
  35.6 1.9 %copy-start.19 = (f32[2048]{0:T(1024)S(1)}, f32[2048]{0:T(1024)}, u32[]{:S(2)}) copy-start(f32[2048]{0:T(1024)} %param.29) | copy-start | bytes 24580
  35.6 1.9 %copy-start.16 = (s32[64,2]{0,1:T(2,128)S(1)}, s32[64,2]{0,1:T(2,128)}, u32[]{:S(2)}) copy-start(s32[64,2]{0,1:T(2,128)} %param.43) | copy-start | bytes 1540
  37.4 81.1 %all-gather.2.cloned.1.call-start = ((), (), s32[]{:S(2)}) async-start(), calls=%async_computation.7 | async-start | bytes 2228224 | tf_op jit(solution)/shard_map/all_gather | solution.py:168
  52.5 75.5 %reduce-scatter.5.cloned.1.call-start = ((), (), s32[]{:S(2)}) async-start(), calls=%async_computation.6 | async-start | bytes 1572864 | tf_op jit(solution)/shard_map/reduce_scatter | solution.py:161
  53.3 44.9 %copy-start.20 = (bf16[1,2048,512]{2,1,0:T(8,128)(2,1)S(1)}, bf16[1,2048,512]{2,1,0:T(8,128)(2,1)}, u32[]{:S(2)}) copy-start(bf16[1,2048,512]{2,1,0:T(8,128)(2,1)} %param.44) | copy-start | bytes 6291460
  97.2 1.0 copy-start.9
  106.9 4.0 %copy-start.17 = (bf16[2048,4]{0,1:T(4,128)(2,1)S(1)}, bf16[2048,4]{0,1:T(4,128)(2,1)}, u32[]{:S(2)}) copy-start(bf16[2048,4]{0,1:T(4,128)(2,1)} %param.40) | copy-start | bytes 49156
  106.9 4.0 %copy-start.15 = (bf16[2048,16]{0,1:T(8,128)(2,1)S(1)}, bf16[2048,16]{0,1:T(8,128)(2,1)}, u32[]{:S(2)}) copy-start(bf16[2048,16]{0,1:T(8,128)(2,1)} %param.41) | copy-start | bytes 196612
  106.9 4.1 %dynamic-slice-start = ((f32[2048]{0:T(1024)}, s32[]{:T(128)}), f32[1024]{0:T(1024)S(1)}, s32[]{:S(2)}) async-start(f32[2048]{0:T(1024)} %param.42, s32[]{:T(128)} %select_n.30), calls=%async_computation.9 | async-start | bytes 8704 | tf_op jit(solution)/shard_map/dynamic_slice | solution.py:88
  106.9 11.6 %copy-start.12 = (bf16[1024,128]{1,0:T(8,128)(2,1)S(1)}, bf16[1024,128]{1,0:T(8,128)(2,1)}, u32[]{:S(2)}) copy-start(bf16[1024,128]{1,0:T(8,128)(2,1)} %param.48) | copy-start | bytes 786436
  111.0 23.9 %copy-start.13 = (bf16[1024,128]{1,0:T(8,128)(2,1)S(1)}, bf16[1024,128]{1,0:T(8,128)(2,1)}, u32[]{:S(2)}) copy-start(bf16[1024,128]{1,0:T(8,128)(2,1)} %param.47) | copy-start | bytes 786436
  128.0 32.3 %all-to-all-start.1 = ((bf16[16,16,1024]{2,1,0:T(8,128)(2,1)}), bf16[16,16,1024]{2,1,0:T(8,128)(2,1)S(1)}, u32[]{:S(2)}, u32[]{:S(2)}) async-start(bf16[16,16,1024]{2,1,0:T(8,128)(2,1)} %bitcast.80), calls=%async_computation.3 | async-start | bytes 1048576 | tf_op jit(solution)/shard_map/all_to_all | solution.py:163
  134.8 23.4 %all-reduce.3.cloned.1.call-start = ((), (), s32[]{:S(2)}) async-start(), calls=%async_computation.8 | async-start | bytes 1048576 | tf_op jit(solution)/shard_map/psum | solution.py:170
  160.3 17.1 %all-to-all-start.2 = ((bf16[16,64,128]{2,1,0:T(8,128)(2,1)}), bf16[16,64,128]{2,1,0:T(8,128)(2,1)S(1)}, u32[]{:S(2)}, u32[]{:S(2)}) async-start(bf16[16,64,128]{2,1,0:T(8,128)(2,1)} %bitcast.19), calls=%async_computation.4 | async-start | bytes 524288 | tf_op jit(solution)/shard_map/all_to_all | solution.py:175
Sparse Core Ops, SparseCore 0:
  37.6 10.4 reduce-scatter.2
  52.6 65.8 all-gather.1
  120.8 7.2 reduce-scatter.4
  138.3 19.8 all-reduce.2
where the time goes:
time: 188 us
  blocking collectives  51.7 us (28%)
  waiting for transfers between devices  49.1 us (26%)
  matrix products  30.9 us (16%)
  local copies, waits for them, and re-layouts  19.7 us (10%)
  between operations  14.3 us (8%)
  starting transfers between devices  13.8 us (7%)
  other arithmetic  8.23 us (4%)
    all_to_all x1, blocking collectives, shards(): lax.all_to_all(outgoing, 'ep', split_axis=0, concat_axis=0, tiled=True)  41 us
    psum x1, waiting for transfers between devices, shards(): lax.psum(partial_dense.astype(jnp.bfloat16), 'tp').astype(jnp.float32)  20 us
    unnamed x49, local copies, waits for them, and re-layouts  15.8 us
    reduce_scatter x1, waiting for transfers between devices, shards(): lax.psum_scatter(stacked.astype(jnp.bfloat16), 'tp', scatter_dimension=2,...  10.3 us
    all_to_all x1, waiting for transfers between devices, shards(): lax.all_to_all(inner_cols, 'ep', split_axis=0, concat_axis=1, tiled=True)  8.24 us
    reduce_scatter x1, waiting for transfers between devices, shards(): lax.psum_scatter(part_out.astype(jnp.bfloat16), 'tp', scatter_dimension=1...  7.08 us
    all_to_all x1, starting transfers between devices, shards(): lax.all_to_all(inner_cols, 'ep', split_axis=0, concat_axis=1, tiled=True)  6.83 us
    all_to_all x1, starting transfers between devices, shards(): lax.all_to_all(finished, 'ep', split_axis=0, concat_axis=0, tiled=True)  6.79 us
  transfers between devices with their start and end apart: 6, of which 5 were waited for; matrix products, arithmetic and copies ran while one was open for 13% of the time, Pallas kernels for 0%

commit v1 on v0

--- a/solution.py
+++ b/solution.py
@@ -6,6 +6,27 @@
 NG = 4
 EPS = 1e-06
 PRECISION_MAX = lax.Precision.HIGHEST
+
+
+def supply_the_zones(payload):
+    axis_tag = "ep"
+    current_block, fresh = (lax.axis_size(axis_tag), lax.axis_index(axis_tag))
+    g_now = payload.shape[0] // current_block
+    piece_out = list(payload.shape)
+    piece_out[0] = g_now
+    lower = piece_out[0]
+    piece_out[0] = lower * current_block
+    seen_now = jnp.zeros(piece_out, payload.dtype)
+    for w in range(current_block):
+        step_out = lax.dynamic_slice_in_dim(payload, (fresh ^ w) * g_now, g_now, axis=0)
+        if w:
+            step_out = lax.ppermute(
+                step_out,
+                axis_tag,
+                list(map(lambda src_i: (src_i, src_i ^ w), range(current_block))),
+            )
+        seen_now = lax.dynamic_update_slice_in_dim(seen_now, step_out, (fresh ^ w) * lower, axis=0)
+    return seen_now
 
 
 def state_factors(rate, freq, log_group_step, input_map_real, input_map_imaginary):
@@ -150,7 +171,7 @@
         dispatch_rows.astype(jnp.bfloat16), full_rows, preferred_element_type=jnp.float32
     )
     outgoing = outgoing.astype(jnp.bfloat16).reshape(experts, capacity, width)
-    received = lax.all_to_all(outgoing, "ep", split_axis=0, concat_axis=0, tiled=True)
+    received = supply_the_zones(outgoing)
     sources = received.shape[0]
     items = received.shape[1]
     token_rows = received.reshape(sources * items, width)

time: 188 us -> 223 us (1.19)
  waiting for transfers between devices: 49.1 us -> 96.6 us
  blocking collectives: 51.7 us -> 10.6 us
  starting transfers between devices: 13.8 us -> 42.7 us
    all_gather x1, waiting for transfers between devices: 3.41 us -> 56.3 us  [shards(): lax.all_gather(hnorm, 'ep', axis=0, tiled=True)]
    all_to_all x1 -> x0, blocking collectives: 41 us -> none  [shards(): lax.all_to_all(outgoing, 'ep', split_axis=0, concat_axis=0, tiled=True)]
    ppermute x0 -> x15, starting transfers between devices: none -> 31.1 us  [supply_the_zones(): lax.ppermute(step_out, axis_tag, list(map(lambda src_i: (src_i, src_i ^ w...]
    reduce_scatter x1, waiting for transfers between devices: 7.08 us -> 0.01 us  [shards(): lax.psum_scatter(part_out.astype(jnp.bfloat16), 'tp', scatter_dimension=1...]
    ppermute x0 -> x15, waiting for transfers between devices: none -> 4.39 us  [supply_the_zones(): lax.ppermute(step_out, axis_tag, list(map(lambda src_i: (src_i, src_i ^ w...]
    psum x1, waiting for transfers between devices: 20 us -> 17.5 us  [shards(): lax.psum(partial_dense.astype(jnp.bfloat16), 'tp').astype(jnp.float32)]
    unnamed x49 -> x53, local copies, waits for them, and re-layouts: 15.8 us -> 16 us
  transfers between devices with their start and end apart: 6 -> 21, of which waited for: 5 -> 6; matrix products, arithmetic and copies ran while one was open for 13% -> 8% of each run, Pallas kernels for 0% -> 0%
where the time goes in v1:
time: 223 us
  waiting for transfers between devices  96.6 us (43%)
  starting transfers between devices  42.7 us (19%)
  matrix products  30.4 us (14%)
  local copies, waits for them, and re-layouts  20.4 us (9%)
  between operations  14.6 us (7%)
  blocking collectives  10.6 us (5%)
  other arithmetic  7.56 us (3%)
    all_gather x1, waiting for transfers between devices, shards(): lax.all_gather(hnorm, 'ep', axis=0, tiled=True)  56.3 us
    ppermute x15, starting transfers between devices, supply_the_zones(): lax.ppermute(step_out, axis_tag, list(map(lambda src_i: (src_i, src_i ^ w...  31.1 us
    psum x1, waiting for transfers between devices, shards(): lax.psum(partial_dense.astype(jnp.bfloat16), 'tp').astype(jnp.float32)  17.5 us
    unnamed x53, local copies, waits for them, and re-layouts  16 us
    reduce_scatter x1, waiting for transfers between devices, shards(): lax.psum_scatter(stacked.astype(jnp.bfloat16), 'tp', scatter_dimension=2,...  9.45 us
    all_to_all x1, waiting for transfers between devices, shards(): lax.all_to_all(inner_cols, 'ep', split_axis=0, concat_axis=1, tiled=True)  8.24 us
    all_to_all x1, starting transfers between devices, shards(): lax.all_to_all(inner_cols, 'ep', split_axis=0, concat_axis=1, tiled=True)  6.83 us
    dot_general x1, matrix products, state_step(): jnp.einsum('tgc,gpc->tgp', grouped, bbar_re, precision=PRECISION_MAX)  4.93 us
  transfers between devices with their start and end apart: 21, of which 6 were waited for; matrix products, arithmetic and copies ran while one was open for 8% of the time, Pallas kernels for 0%

profile of v1, /device:TPU:0, one launch (start us, length us, event | category | flops | bytes accessed | tf_op | source)
XLA Modules:
  0.0 222.8 jit_solution(11777853794460047601)
XLA Ops:
  7.2 3.5 %copy.64 = f32[64,64,64]{0,2,1:T(8,128)} copy(f32[64,64,64]{2,1,0:T(8,128)} %param.27) | data formatting | bytes 2097152 | tf_op args[2]
  10.7 3.4 %copy.63 = f32[64,64,64]{0,2,1:T(8,128)} copy(f32[64,64,64]{2,1,0:T(8,128)} %param.26) | data formatting | bytes 2097152 | tf_op args[1]
  14.3 2.6 %psum.35 = f32[64]{0:T(128)S(1)} all-reduce(f32[64]{0:T(128)S(1)} %fusion.16), channel_id=1, replica_groups=mesh['ep'=16,'tp'=2] {'tp'}, use_global_device_ids=true, to_apply=%region_1.0 | all-reduce | flops 64 | bytes 512 | tf_op jit(solution)/shard_map/psum | solution.py:112
  19.8 4.9 %bitcast_add_fusion.1 = f32[64,64,64]{0,2,1:T(8,128)S(1)} fusion(f32[64,64,64]{0,2,1:T(8,128)} %copy.64, f32[64,64,64]{0,2,1:T(8,128)} %copy.63, bf16[64,64,16]{0,2,1:T(8,128)(2,1)S(1)} %bitcast.73, f32[64,64]{1,0:T(8,128)S(1)} %get-tuple-element.33, f32[64,64]{1,0:T(8,128)S(1)} %get-tuple-element.34, f32[64,64,16]{1,2,0:T(8,128)S(1)} %copy-done.8, ...), kind=kOutput, calls=%fused_computation.13 | convolution fusion | flops 51576832 | bytes 3866624 | tf_op jit(solution)/shard_map/tgc,gpc->tgp/dot_general | solution.py:59
  24.8 3.2 %bitcast_add_fusion = f32[64,64,64]{0,2,1:T(8,128)S(1)} fusion(f32[64,64,64]{0,2,1:T(8,128)S(1)} %copy-done.4, f32[64,64,64]{0,2,1:T(8,128)S(1)} %copy-done.3, bf16[64,64,16]{0,2,1:T(8,128)(2,1)S(1)} %bitcast.74, f32[64,64]{1,0:T(8,128)S(1)} %get-tuple-element.33, f32[64,64]{1,0:T(8,128)S(1)} %get-tuple-element.34, f32[64,64,16]{1,2,0:T(8,128)S(1)} %copy-done.9, ...), kind=kOutput, calls=%fused_computation.12 | convolution fusion | flops 51576832 | bytes 3866624 | tf_op jit(solution)/shard_map/tgc,gpc->tgp/dot_general | solution.py:60
  28.1 1.9 fusion.68
  30.0 1.9 convolution_subtract_fusion
  32.1 3.3 %fusion.1 = bf16[64,1,2048]{2,0,1:T(8,128)(2,1)S(1)} fusion(bf16[1024,2048]{1,0:T(8,128)(2,1)} %param.39, f32[64,1024]{1,0:T(8,128)S(1)} %copy.70, f32[1024]{0:T(1024)S(1)} %copy-done.16, f32[1024]{0:T(1024)S(1)} %dynamic_slice.63, f32[64]{0:T(128)S(1)} %add_rsqrt_fusion.1, bf16[64,1024]{1,0:T(8,128)(2,1)S(1)} %copy-done.7), kind=kOutput, calls=%fused_computation.6 | convolution fusion | flops 269615104 | bytes 4858112 | tf_op jit(solution)/shard_map/dot_general | solution.py:127
  38.6 9.5 %reduce-scatter.3.cloned.1.call-done = bf16[64,2,1024]{2,0,1:T(8,128)(2,1)} async-done(((bf16[64,2,2048]{2,0,1:T(8,128)(2,1)}), bf16[64,2,1024]{2,0,1:T(8,128)(2,1)}) %reduce-scatter.3.cloned.1.call-update) | async-done | bytes 262160 | tf_op jit(solution)/shard_map/reduce_scatter | solution.py:129
  49.3 2.5 %psum.36 = f32[64]{0:T(128)S(1)} all-reduce(f32[64]{0:T(128)S(1)} %get-tuple-element.14), channel_id=1, replica_groups=mesh['ep'=16,'tp'=2] {'tp'}, use_global_device_ids=true, to_apply=%region_4.0 | all-reduce | flops 64 | bytes 512 | tf_op jit(solution)/shard_map/psum | solution.py:141
  51.9 2.2 all_gather.6
  54.8 1.8 collective-permute-start
  58.4 1.7 collective-permute-start.3
  61.5 2.4 %collective-permute-start.5 = (bf16[1,16,2048]{2,1,0:T(8,128)(2,1)S(1)}, bf16[1,16,2048]{2,1,0:T(8,128)(2,1)S(1)}, u32[]{:S(2)}, u32[]{:S(2)}) collective-permute-start(bf16[1,16,2048]{2,1,0:T(8,128)(2,1)S(1)} %get-tuple-element.25), channel_id=1, source_target_pairs={{0,12},{2,14},{4,8},{6,10},{8,4},{10,6},{12,0},{14,2},{16,28},{18,... | collective-permute-start | bytes 196616 | tf_op jit(solution)/shard_map/ppermute | solution.py:23
  64.3 2.7 %collective-permute-start.7 = (bf16[1,16,2048]{2,1,0:T(8,128)(2,1)S(1)}, bf16[1,16,2048]{2,1,0:T(8,128)(2,1)S(1)}, u32[]{:S(2)}, u32[]{:S(2)}) collective-permute-start(bf16[1,16,2048]{2,1,0:T(8,128)(2,1)S(1)} %get-tuple-element.23), channel_id=1, source_target_pairs={{0,16},{2,18},{4,20},{6,22},{8,24},{10,26},{12,28},{14,30},{16,0},... | collective-permute-start | bytes 196616 | tf_op jit(solution)/shard_map/ppermute | solution.py:23
  68.6 3.4 %collective-permute-start.9 = (bf16[1,16,2048]{2,1,0:T(8,128)(2,1)S(1)}, bf16[1,16,2048]{2,1,0:T(8,128)(2,1)S(1)}, u32[]{:S(2)}, u32[]{:S(2)}) collective-permute-start(bf16[1,16,2048]{2,1,0:T(8,128)(2,1)S(1)} %get-tuple-element.21), channel_id=1, source_target_pairs={{0,20},{2,22},{4,16},{6,18},{8,28},{10,30},{12,24},{14,26},{16,4},... | collective-permute-start | bytes 196616 | tf_op jit(solution)/shard_map/ppermute | solution.py:23
  72.3 3.6 %collective-permute-start.11 = (bf16[1,16,2048]{2,1,0:T(8,128)(2,1)S(1)}, bf16[1,16,2048]{2,1,0:T(8,128)(2,1)S(1)}, u32[]{:S(2)}, u32[]{:S(2)}) collective-permute-start(bf16[1,16,2048]{2,1,0:T(8,128)(2,1)S(1)} %get-tuple-element.19), channel_id=1, source_target_pairs={{0,24},{2,26},{4,28},{6,30},{8,16},{10,18},{12,20},{14,22},{16,8},... | collective-permute-start | bytes 196616 | tf_op jit(solution)/shard_map/ppermute | solution.py:23
  76.0 2.3 %collective-permute-start.12 = (bf16[1,16,2048]{2,1,0:T(8,128)(2,1)S(1)}, bf16[1,16,2048]{2,1,0:T(8,128)(2,1)S(1)}, u32[]{:S(2)}, u32[]{:S(2)}) collective-permute-start(bf16[1,16,2048]{2,1,0:T(8,128)(2,1)S(1)} %get-tuple-element.18), channel_id=1, source_target_pairs={{0,26},{2,24},{4,30},{6,28},{8,18},{10,16},{12,22},{14,20},{16,10}... | collective-permute-start | bytes 196616 | tf_op jit(solution)/shard_map/ppermute | solution.py:23
  78.2 4.3 %collective-permute-start.13 = (bf16[1,16,2048]{2,1,0:T(8,128)(2,1)S(1)}, bf16[1,16,2048]{2,1,0:T(8,128)(2,1)S(1)}, u32[]{:S(2)}, u32[]{:S(2)}) collective-permute-start(bf16[1,16,2048]{2,1,0:T(8,128)(2,1)S(1)} %get-tuple-element.17), channel_id=1, source_target_pairs={{0,28},{2,30},{4,24},{6,26},{8,20},{10,22},{12,16},{14,18},{16,12}... | collective-permute-start | bytes 196616 | tf_op jit(solution)/shard_map/ppermute | solution.py:23
  82.6 3.6 %collective-permute-start.14 = (bf16[1,16,2048]{2,1,0:T(8,128)(2,1)S(1)}, bf16[1,16,2048]{2,1,0:T(8,128)(2,1)S(1)}, u32[]{:S(2)}, u32[]{:S(2)}) collective-permute-start(bf16[1,16,2048]{2,1,0:T(8,128)(2,1)S(1)} %get-tuple-element.16), channel_id=1, source_target_pairs={{0,30},{2,28},{4,26},{6,24},{8,22},{10,20},{12,18},{14,16},{16,14}... | collective-permute-start | bytes 196616 | tf_op jit(solution)/shard_map/ppermute | solution.py:23
  86.4 4.2 %collective-permute-done.14 = bf16[1,16,2048]{2,1,0:T(8,128)(2,1)S(1)} collective-permute-done((bf16[1,16,2048]{2,1,0:T(8,128)(2,1)S(1)}, bf16[1,16,2048]{2,1,0:T(8,128)(2,1)S(1)}, u32[]{:S(2)}, u32[]{:S(2)}) %collective-permute-start.14) | collective-permute-done | bytes 65568 | tf_op jit(solution)/shard_map/ppermute | solution.py:23
  93.1 4.4 %convolution_convert_fusion = bf16[256,2048]{1,0:T(8,128)(2,1)} fusion(bf16[1,512,2048]{2,1,0:T(8,128)(2,1)S(1)} %copy-done, f32[256,512]{1,0:T(8,128)} %fusion.3, bf16[256,2048]{1,0:T(8,128)(2,1)} %bitcast.77, bf16[1,2048,512]{2,1,0:T(8,128)(2,1)} %param.44), kind=kOutput, calls=%fused_computation.1 | convolution fusion | flops 1075052544 | bytes 6815744 | tf_op jit(solution)/shard_map/dot_general | solution.py:181
  98.2 3.8 %copy.77 = f32[64,64,64]{2,1,0:T(8,128)} copy(f32[64,64,64]{0,2,1:T(8,128)} %copy-done.2) | data formatting | bytes 2097152
  102.0 4.1 %copy.78 = f32[64,64,64]{2,1,0:T(8,128)} copy(f32[64,64,64]{0,2,1:T(8,128)} %copy-done.1) | data formatting | bytes 2097152
  107.1 3.3 %all-reduce = (f32[64,20]{0,1:T(8,128)S(1)}, f32[64]{0:T(128)S(1)}) all-reduce(f32[64,20]{0,1:T(8,128)S(1)} %fusion.31, f32[64]{0:T(128)S(1)} %convolution_bitcast_fusion), channel_id=1, replica_groups=mesh['ep'=16,'tp'=2] {'tp'}, use_global_device_ids=true, to_apply=%region_5.0 | all-reduce | flops 1344 | bytes 10752 | tf_op jit(solution)/shard_map/psum | solution.py:146
  110.5 4.6 %all-to-all-start = ((bf16[16,16,1024]{2,1,0:T(8,128)(2,1)}), bf16[16,16,1024]{2,1,0:T(8,128)(2,1)S(1)}, u32[]{:S(2)}, u32[]{:S(2)}) async-start(bf16[16,16,1024]{2,1,0:T(8,128)(2,1)} %bitcast.79), calls=%async_computation.2 | async-start | bytes 1048576 | tf_op jit(solution)/shard_map/all_to_all | solution.py:184
  115.1 56.3 %all-gather.2.cloned.1.call-done = bf16[1024,1024]{1,0:T(8,128)(2,1)} async-done(((bf16[64,1024]{1,0:T(8,128)(2,1)}), bf16[1024,1024]{1,0:T(8,128)(2,1)}) %all-gather.2.cloned.1.call-update) | async-done | bytes 2097168 | tf_op jit(solution)/shard_map/all_gather | solution.py:189
  171.5 2.6 %convolution_convert_fusion.4 = bf16[1024,128]{0,1:T(8,128)(2,1)S(1)} fusion(bf16[1024,1024]{1,0:T(8,128)(2,1)} %all-gather.2.cloned.1.call-done, bf16[1024,128]{1,0:T(8,128)(2,1)S(1)} %copy-done.14), kind=kOutput, calls=%fused_computation.15 | convolution fusion | flops 268566528 | bytes 2621440 | tf_op jit(solution)/shard_map/dot_general | solution.py:73
  175.8 17.5 %all-reduce.3.cloned.1.call-done = bf16[1024,256]{0,1:T(8,128)(2,1)} async-done(((bf16[1024,256]{0,1:T(8,128)(2,1)}), bf16[1024,256]{0,1:T(8,128)(2,1)}) %all-reduce.3.cloned.1.call-update) | async-done | bytes 524304 | tf_op jit(solution)/shard_map/psum | solution.py:191
  195.5 6.8 %all-to-all-start.1 = ((bf16[16,64,128]{2,1,0:T(8,128)(2,1)}), bf16[16,64,128]{2,1,0:T(8,128)(2,1)S(1)}, u32[]{:S(2)}, u32[]{:S(2)}) async-start(bf16[16,64,128]{2,1,0:T(8,128)(2,1)} %bitcast.78), calls=%async_computation.3 | async-start | bytes 524288 | tf_op jit(solution)/shard_map/all_to_all | solution.py:196
  204.3 8.2 %all-to-all-done.1 = bf16[16,64,128]{2,1,0:T(8,128)(2,1)S(1)} async-done(((bf16[16,64,128]{2,1,0:T(8,128)(2,1)}), bf16[16,64,128]{2,1,0:T(8,128)(2,1)S(1)}, u32[]{:S(2)}, u32[]{:S(2)}) %all-to-all-start.1) | async-done | bytes 262176 | tf_op jit(solution)/shard_map/all_to_all | solution.py:196
  212.6 3.7 %fusion.8 = bf16[64,1024]{1,0:T(8,128)(2,1)} fusion(bf16[2048,1024]{1,0:T(8,128)(2,1)} %param.49, f32[64,1024]{1,0:T(8,128)S(1)} %multiply_reduce_fusion, bf16[64,1024]{1,0:T(8,128)(2,1)S(1)} %get-tuple-element.15, f32[64]{0:T(128)S(1)} %add_divide_fusion, bf16[16,64,128]{2,1,0:T(8,128)(2,1)S(1)} %all-to-all-done.1), kind=kOutput, calls=%fused_computation.19 | convolution fusion | flops 268763136 | bytes 4980992 | tf_op jit(solution)/shard_map/dot_general | solution.py:197
  (151 shorter events, 24.2 us)
Async XLA Ops:
  7.2 86.0 %copy-start = (bf16[1,512,2048]{2,1,0:T(8,128)(2,1)S(1)}, bf16[1,512,2048]{2,1,0:T(8,128)(2,1)}, u32[]{:S(2)}) copy-start(bf16[1,512,2048]{2,1,0:T(8,128)(2,1)} %param.46) | copy-start | bytes 6291460
  7.2 40.9 %reduce-scatter.3.cloned.1.call-start = ((), (), s32[]{:S(2)}) async-start(), calls=%async_computation.4 | async-start | bytes 786432 | tf_op jit(solution)/shard_map/reduce_scatter | solution.py:129
  10.7 6.2 %copy-start.20 = (f32[2048]{0:T(1024)S(1)}, f32[2048]{0:T(1024)}, u32[]{:S(2)}) copy-start(f32[2048]{0:T(1024)} %param.28) | copy-start | bytes 24580
  10.7 8.0 %copy-start.23 = (f32[64]{0:T(128)S(1)}, f32[64]{0:T(128)}, u32[]{:S(2)}) copy-start(f32[64]{0:T(128)} %param.32) | copy-start | bytes 772
  10.7 9.1 %copy-start.8 = (f32[64,64,16]{1,2,0:T(8,128)S(1)}, f32[64,64,16]{1,2,0:T(8,128)}, u32[]{:S(2)}) copy-start(f32[64,64,16]{1,2,0:T(8,128)} %param.34) | copy-start | bytes 786436
  10.7 9.1 %copy-start.9 = (f32[64,64,16]{1,2,0:T(8,128)S(1)}, f32[64,64,16]{1,2,0:T(8,128)}, u32[]{:S(2)}) copy-start(f32[64,64,16]{1,2,0:T(8,128)} %param.33) | copy-start | bytes 786436
  19.8 5.0 %copy-start.3 = (f32[64,64,64]{0,2,1:T(8,128)S(1)}, f32[64,64,64]{0,2,1:T(8,128)}, u32[]{:S(2)}) copy-start(f32[64,64,64]{0,2,1:T(8,128)} %copy.64) | copy-start | bytes 3145732
  19.8 5.0 %copy-start.4 = (f32[64,64,64]{0,2,1:T(8,128)S(1)}, f32[64,64,64]{0,2,1:T(8,128)}, u32[]{:S(2)}) copy-start(f32[64,64,64]{0,2,1:T(8,128)} %copy.63) | copy-start | bytes 3145732
  37.4 73.0 %reduce-scatter.5.cloned.1.call-start = ((), (), s32[]{:S(2)}) async-start(), calls=%async_computation.5 | async-start | bytes 1572864 | tf_op jit(solution)/shard_map/reduce_scatter | solution.py:182
  54.6 37.0 %copy-start.22 = (bf16[1,2048,512]{2,1,0:T(8,128)(2,1)S(1)}, bf16[1,2048,512]{2,1,0:T(8,128)(2,1)}, u32[]{:S(2)}) copy-start(bf16[1,2048,512]{2,1,0:T(8,128)(2,1)} %param.45) | copy-start | bytes 6291460
  54.8 6.7 %collective-permute-start = (bf16[1,16,2048]{2,1,0:T(8,128)(2,1)S(1)}, bf16[1,16,2048]{2,1,0:T(8,128)(2,1)S(1)}, u32[]{:S(2)}, u32[]{:S(2)}) collective-permute-start(bf16[1,16,2048]{2,1,0:T(8,128)(2,1)S(1)} %get-tuple-element.30), channel_id=1, source_target_pairs={{0,2},{2,0},{4,6},{6,4},{8,10},{10,8},{12,14},{14,12},{16,18},{18,... | collective-permute-start | bytes 196616 | tf_op jit(solution)/shard_map/ppermute | solution.py:23
  56.6 7.4 %collective-permute-start.1 = (bf16[1,16,2048]{2,1,0:T(8,128)(2,1)S(1)}, bf16[1,16,2048]{2,1,0:T(8,128)(2,1)S(1)}, u32[]{:S(2)}, u32[]{:S(2)}) collective-permute-start(bf16[1,16,2048]{2,1,0:T(8,128)(2,1)S(1)} %get-tuple-element.29), channel_id=1, source_target_pairs={{0,4},{2,6},{4,0},{6,2},{8,12},{10,14},{12,8},{14,10},{16,20},{18,... | collective-permute-start | bytes 196616 | tf_op jit(solution)/shard_map/ppermute | solution.py:23
  58.0 6.3 %collective-permute-start.2 = (bf16[1,16,2048]{2,1,0:T(8,128)(2,1)S(1)}, bf16[1,16,2048]{2,1,0:T(8,128)(2,1)S(1)}, u32[]{:S(2)}, u32[]{:S(2)}) collective-permute-start(bf16[1,16,2048]{2,1,0:T(8,128)(2,1)S(1)} %get-tuple-element.28), channel_id=1, source_target_pairs={{0,6},{2,4},{4,2},{6,0},{8,14},{10,12},{12,10},{14,8},{16,22},{18,... | collective-permute-start | bytes 196616 | tf_op jit(solution)/shard_map/ppermute | solution.py:23
  58.4 8.7 %collective-permute-start.3 = (bf16[1,16,2048]{2,1,0:T(8,128)(2,1)S(1)}, bf16[1,16,2048]{2,1,0:T(8,128)(2,1)S(1)}, u32[]{:S(2)}, u32[]{:S(2)}) collective-permute-start(bf16[1,16,2048]{2,1,0:T(8,128)(2,1)S(1)} %get-tuple-element.27), channel_id=1, source_target_pairs={{0,8},{2,10},{4,12},{6,14},{8,0},{10,2},{12,4},{14,6},{16,24},{18,... | collective-permute-start | bytes 196616 | tf_op jit(solution)/shard_map/ppermute | solution.py:23
  60.1 8.5 %collective-permute-start.4 = (bf16[1,16,2048]{2,1,0:T(8,128)(2,1)S(1)}, bf16[1,16,2048]{2,1,0:T(8,128)(2,1)S(1)}, u32[]{:S(2)}, u32[]{:S(2)}) collective-permute-start(bf16[1,16,2048]{2,1,0:T(8,128)(2,1)S(1)} %get-tuple-element.26), channel_id=1, source_target_pairs={{0,10},{2,8},{4,14},{6,12},{8,2},{10,0},{12,6},{14,4},{16,26},{18,... | collective-permute-start | bytes 196616 | tf_op jit(solution)/shard_map/ppermute | solution.py:23
  61.5 10.4 %collective-permute-start.5 = (bf16[1,16,2048]{2,1,0:T(8,128)(2,1)S(1)}, bf16[1,16,2048]{2,1,0:T(8,128)(2,1)S(1)}, u32[]{:S(2)}, u32[]{:S(2)}) collective-permute-start(bf16[1,16,2048]{2,1,0:T(8,128)(2,1)S(1)} %get-tuple-element.25), channel_id=1, source_target_pairs={{0,12},{2,14},{4,8},{6,10},{8,4},{10,6},{12,0},{14,2},{16,28},{18,... | collective-permute-start | bytes 196616 | tf_op jit(solution)/shard_map/ppermute | solution.py:23
  63.9 8.4 %collective-permute-start.6 = (bf16[1,16,2048]{2,1,0:T(8,128)(2,1)S(1)}, bf16[1,16,2048]{2,1,0:T(8,128)(2,1)S(1)}, u32[]{:S(2)}, u32[]{:S(2)}) collective-permute-start(bf16[1,16,2048]{2,1,0:T(8,128)(2,1)S(1)} %get-tuple-element.24), channel_id=1, source_target_pairs={{0,14},{2,12},{4,10},{6,8},{8,6},{10,4},{12,2},{14,0},{16,30},{18,... | collective-permute-start | bytes 196616 | tf_op jit(solution)/shard_map/ppermute | solution.py:23
  64.3 11.6 %collective-permute-start.7 = (bf16[1,16,2048]{2,1,0:T(8,128)(2,1)S(1)}, bf16[1,16,2048]{2,1,0:T(8,128)(2,1)S(1)}, u32[]{:S(2)}, u32[]{:S(2)}) collective-permute-start(bf16[1,16,2048]{2,1,0:T(8,128)(2,1)S(1)} %get-tuple-element.23), channel_id=1, source_target_pairs={{0,16},{2,18},{4,20},{6,22},{8,24},{10,26},{12,28},{14,30},{16,0},... | collective-permute-start | bytes 196616 | tf_op jit(solution)/shard_map/ppermute | solution.py:23
  67.0 11.2 %collective-permute-start.8 = (bf16[1,16,2048]{2,1,0:T(8,128)(2,1)S(1)}, bf16[1,16,2048]{2,1,0:T(8,128)(2,1)S(1)}, u32[]{:S(2)}, u32[]{:S(2)}) collective-permute-start(bf16[1,16,2048]{2,1,0:T(8,128)(2,1)S(1)} %get-tuple-element.22), channel_id=1, source_target_pairs={{0,18},{2,16},{4,22},{6,20},{8,26},{10,24},{12,30},{14,28},{16,2},... | collective-permute-start | bytes 196616 | tf_op jit(solution)/shard_map/ppermute | solution.py:23
  68.6 14.0 %collective-permute-start.9 = (bf16[1,16,2048]{2,1,0:T(8,128)(2,1)S(1)}, bf16[1,16,2048]{2,1,0:T(8,128)(2,1)S(1)}, u32[]{:S(2)}, u32[]{:S(2)}) collective-permute-start(bf16[1,16,2048]{2,1,0:T(8,128)(2,1)S(1)} %get-tuple-element.21), channel_id=1, source_target_pairs={{0,20},{2,22},{4,16},{6,18},{8,28},{10,30},{12,24},{14,26},{16,4},... | collective-permute-start | bytes 196616 | tf_op jit(solution)/shard_map/ppermute | solution.py:23
  72.0 14.4 %collective-permute-start.10 = (bf16[1,16,2048]{2,1,0:T(8,128)(2,1)S(1)}, bf16[1,16,2048]{2,1,0:T(8,128)(2,1)S(1)}, u32[]{:S(2)}, u32[]{:S(2)}) collective-permute-start(bf16[1,16,2048]{2,1,0:T(8,128)(2,1)S(1)} %get-tuple-element.20), channel_id=1, source_target_pairs={{0,22},{2,20},{4,18},{6,16},{8,30},{10,28},{12,26},{14,24},{16,6},... | collective-permute-start | bytes 196616 | tf_op jit(solution)/shard_map/ppermute | solution.py:23
  72.3 14.0 %collective-permute-start.11 = (bf16[1,16,2048]{2,1,0:T(8,128)(2,1)S(1)}, bf16[1,16,2048]{2,1,0:T(8,128)(2,1)S(1)}, u32[]{:S(2)}, u32[]{:S(2)}) collective-permute-start(bf16[1,16,2048]{2,1,0:T(8,128)(2,1)S(1)} %get-tuple-element.19), channel_id=1, source_target_pairs={{0,24},{2,26},{4,28},{6,30},{8,16},{10,18},{12,20},{14,22},{16,8},... | collective-permute-start | bytes 196616 | tf_op jit(solution)/shard_map/ppermute | solution.py:23
  76.0 10.4 %collective-permute-start.12 = (bf16[1,16,2048]{2,1,0:T(8,128)(2,1)S(1)}, bf16[1,16,2048]{2,1,0:T(8,128)(2,1)S(1)}, u32[]{:S(2)}, u32[]{:S(2)}) collective-permute-start(bf16[1,16,2048]{2,1,0:T(8,128)(2,1)S(1)} %get-tuple-element.18), channel_id=1, source_target_pairs={{0,26},{2,24},{4,30},{6,28},{8,18},{10,16},{12,22},{14,20},{16,10}... | collective-permute-start | bytes 196616 | tf_op jit(solution)/shard_map/ppermute | solution.py:23
  78.2 8.2 %collective-permute-start.13 = (bf16[1,16,2048]{2,1,0:T(8,128)(2,1)S(1)}, bf16[1,16,2048]{2,1,0:T(8,128)(2,1)S(1)}, u32[]{:S(2)}, u32[]{:S(2)}) collective-permute-start(bf16[1,16,2048]{2,1,0:T(8,128)(2,1)S(1)} %get-tuple-element.17), channel_id=1, source_target_pairs={{0,28},{2,30},{4,24},{6,26},{8,20},{10,22},{12,16},{14,18},{16,12}... | collective-permute-start | bytes 196616 | tf_op jit(solution)/shard_map/ppermute | solution.py:23
  82.6 8.0 %collective-permute-start.14 = (bf16[1,16,2048]{2,1,0:T(8,128)(2,1)S(1)}, bf16[1,16,2048]{2,1,0:T(8,128)(2,1)S(1)}, u32[]{:S(2)}, u32[]{:S(2)}) collective-permute-start(bf16[1,16,2048]{2,1,0:T(8,128)(2,1)S(1)} %get-tuple-element.16), channel_id=1, source_target_pairs={{0,30},{2,28},{4,26},{6,24},{8,22},{10,20},{12,18},{14,16},{16,14}... | collective-permute-start | bytes 196616 | tf_op jit(solution)/shard_map/ppermute | solution.py:23
  97.5 74.0 %all-gather.2.cloned.1.call-start = ((), (), s32[]{:S(2)}) async-start(), calls=%async_computation.6 | async-start | bytes 2228224 | tf_op jit(solution)/shard_map/all_gather | solution.py:189
  102.0 4.3 %dynamic-slice-start = ((f32[2048]{0:T(1024)}, s32[]{:T(128)}), f32[1024]{0:T(1024)S(1)}, s32[]{:S(2)}) async-start(f32[2048]{0:T(1024)} %param.42, s32[]{:T(128)} %select_n.94), calls=%async_computation.8 | async-start | bytes 8704 | tf_op jit(solution)/shard_map/dynamic_slice | solution.py:109
  102.0 69.4 %copy-start.14 = (bf16[1024,128]{1,0:T(8,128)(2,1)S(1)}, bf16[1024,128]{1,0:T(8,128)(2,1)}, u32[]{:S(2)}) copy-start(bf16[1024,128]{1,0:T(8,128)(2,1)} %param.48) | copy-start | bytes 786436
  106.3 67.7 %copy-start.15 = (bf16[1024,128]{1,0:T(8,128)(2,1)S(1)}, bf16[1024,128]{1,0:T(8,128)(2,1)}, u32[]{:S(2)}) copy-start(bf16[1024,128]{1,0:T(8,128)(2,1)} %param.47) | copy-start | bytes 786436
  110.5 85.0 %all-to-all-start = ((bf16[16,16,1024]{2,1,0:T(8,128)(2,1)}), bf16[16,16,1024]{2,1,0:T(8,128)(2,1)S(1)}, u32[]{:S(2)}, u32[]{:S(2)}) async-start(bf16[16,16,1024]{2,1,0:T(8,128)(2,1)} %bitcast.79), calls=%async_computation.2 | async-start | bytes 1048576 | tf_op jit(solution)/shard_map/all_to_all | solution.py:184
  115.1 78.2 %all-reduce.3.cloned.1.call-start = ((), (), s32[]{:S(2)}) async-start(), calls=%async_computation.7 | async-start | bytes 1048576 | tf_op jit(solution)/shard_map/psum | solution.py:191
  195.5 17.1 %all-to-all-start.1 = ((bf16[16,64,128]{2,1,0:T(8,128)(2,1)}), bf16[16,64,128]{2,1,0:T(8,128)(2,1)S(1)}, u32[]{:S(2)}, u32[]{:S(2)}) async-start(bf16[16,64,128]{2,1,0:T(8,128)(2,1)} %bitcast.78), calls=%async_computation.3 | async-start | bytes 524288 | tf_op jit(solution)/shard_map/all_to_all | solution.py:196
  (14 other events, 40.4 us)
Sparse Core Ops, SparseCore 0:
  37.6 10.4 reduce-scatter.2
  97.6 7.5 reduce-scatter.4
  108.6 62.7 all-gather.1
  175.9 17.3 all-reduce.2
